TPU v7x, 32 devices: a whole 2x2x4 slice. The times are simulated.
32 devices in a mesh: sp: 16 (over z, y, x), tp: 2 (over core).
Axes of the slice: x: 2, y: 2, z: 4, core: 2. Of those that a mesh axis runs over, the one named last changes fastest.
Arguments:
- layer_source_tokens: bfloat16 [2, 1024, 4096], P(None, 'sp'), may hold values from -6 to 6
- address_projection: bfloat16 [4096, 2048], P('sp', 'tp'), may hold values from -0.09375 to 0.09375
- content_projection: bfloat16 [4096, 2048], P('sp', 'tp'), may hold values from -0.09375 to 0.09375
- strength_projection: bfloat16 [4096, 16], replicated, may hold values from -0.09375 to 0.09375
- fading_driver_projection: bfloat16 [4096, 16], replicated, may hold values from -0.25 to 0.25
- strength_offset: float32 [16], P('tp'), may hold values from -2.5 to 1
- channel_fading_speed: float32 [16], P('tp')
- added_fading_exponent: float32 [2, 1024, 16], P(None, 'sp', 'tp'), may hold values from -0.7 to 0, as said below
- first_step_probe: bfloat16 [2, 2048], P(None, 'tp'), may hold values from -6 to 6
- first_step_address: bfloat16 [2, 2048], P(None, 'tp'), may hold values from -6 to 6
- first_step_content: bfloat16 [2, 2048], P(None, 'tp'), may hold values from -6 to 6
- first_step_outgate: bfloat16 [2, 2048], P(None, 'tp'), may hold values from -6 to 6
- first_step_strength_raw: float32 [2, 16], P(None, 'tp'), may hold values from -6 to 6
- channel_scaling_factor: float32 [128], replicated, may hold values from 0.1 to 1.9
- readout_projection: bfloat16 [2048, 4096], P('tp', 'sp'), may hold values from -0.125 to 0.125
Outputs:
- state_cache: bfloat16 [2, 16, 128, 128], P(None, 'tp')
- mixed_read: bfloat16 [2, 4096], P(None, 'sp')
- boundary_cache: bfloat16 [2, 16, 16, 128, 128], P(None, 'sp', 'tp')
Inputs may be any that keep to these rules, and one draw needn't show every extreme that they name: `added_fading_exponent`: zero at most positions.
All inputs are finite; a program needn't handle non-finite values.
Results may differ from a plain program's by a relative error of at most 0.017.
Values may be sent and summed in bfloat16 or wider, within the bound.
A program may use at most 64 MiB of HBM per device.

v0:
```python
import jax
import jax.numpy as jnp
from jax import lax
from jax.sharding import PartitionSpec as P

ADDRESS_WIDTH = 128
BLOCK = 64


EPSILON = 1e-06
HIGHEST_ACCURACY = lax.Precision.HIGHEST


def prefix(array, axis, combine, identity):
    peers, index = (lax.axis_size(axis), lax.axis_index(axis))
    everything = jax.tree.map(
        lambda part, kind: lax.all_gather(part.astype(kind), axis),
        array,
        (jnp.bfloat16, jnp.bfloat16),
    )
    start = jax.tree.map(
        lambda part, zero: jnp.broadcast_to(jnp.asarray(zero, part.dtype), part.shape),
        array,
        identity,
    )

    def step(k, before):
        reached = k < index
        new = combine(
            before, jax.tree.map(lambda part, own: part[k].astype(own.dtype), everything, array)
        )
        return jax.tree.map(lambda a, b: jnp.where(reached, a, b), new, before)

    return lax.fori_loop(0, peers, step, start)


def as_sent(array):
    return jax.tree.map(lambda a: a.astype(jnp.bfloat16) if a.dtype == jnp.float32 else a, array)


def broadcast(value, axis, source):
    kept = jnp.where(lax.axis_index(axis) == source, value, 0).astype(value.dtype)
    return lax.psum(kept, axis)


def unit_inverse(lower_part):
    matrix_order = lower_part.shape[-1]
    identity = jnp.eye(matrix_order, dtype=jnp.float32)
    result = identity - lower_part
    power_term = lower_part
    reached = 2
    while reached < matrix_order:
        power_term = jnp.matmul(power_term, power_term, precision=HIGHEST_ACCURACY)
        result = jnp.matmul(result, identity + power_term, precision=HIGHEST_ACCURACY)
        reached = reached * 2
    return result


def build_arguments(
    address_vectors,
    content_vectors,
    outgate_raw_scores,
    strength_offset,
    channel_fading_speed,
    added_fading_exponent,
    channel_width,
):
    length = address_vectors.shape[0]
    attention_channels_total = channel_fading_speed.shape[0]
    address_token_slab = jax.nn.silu(address_vectors.astype(jnp.float32)).reshape(
        length, attention_channels_total, channel_width
    )
    address_token_slab = address_token_slab * lax.rsqrt(
        jnp.sum(address_token_slab * address_token_slab, axis=-1, keepdims=True) + EPSILON
    )
    content_token_slab = jax.nn.silu(content_vectors.astype(jnp.float32)).reshape(
        length, attention_channels_total, channel_width
    )
    strength_raw_expanded = outgate_raw_scores.astype(jnp.float32)
    storing_strength = jax.nn.sigmoid(
        strength_raw_expanded[:, :attention_channels_total] + strength_offset
    )
    fading_exponent = added_fading_exponent - channel_fading_speed * jax.nn.softplus(
        strength_raw_expanded[:, attention_channels_total:]
    )
    return (address_token_slab, content_token_slab, storing_strength, fading_exponent)


def range_map(address_token_slab, content_token_slab, storing_strength, fading_exponent, block):
    length, attention_channels_total, channel_width = address_token_slab.shape
    blocks = length // block

    def split_blocks(tensor):
        moved_axes = jnp.swapaxes(tensor, 0, 1)
        return moved_axes.reshape((attention_channels_total, blocks, block) + moved_axes.shape[2:])

    block_keys = split_blocks(address_token_slab)
    block_values = split_blocks(content_token_slab)
    block_beta = split_blocks(storing_strength)
    cumulative = jnp.cumsum(split_blocks(fading_exponent), axis=-1)
    positions = jnp.arange(block)
    strict = positions[:, None] > positions[None, :]
    spread_log = jnp.where(strict, cumulative[..., :, None] - cumulative[..., None, :], 0.0)
    scaled_keys = block_keys * block_beta[..., None]
    inner_prod = jnp.einsum("hnik,hnjk->hnij", scaled_keys, block_keys, precision=HIGHEST_ACCURACY)
    lower_part = jnp.where(strict, inner_prod * jnp.exp(spread_log), 0.0)
    inverse = unit_inverse(lower_part)
    targets = jnp.concatenate(
        [block_values * block_beta[..., None], scaled_keys * jnp.exp(cumulative)[..., None]],
        axis=-1,
    )
    solved = jnp.einsum("hnij,hnjk->hnik", inverse, targets, precision=HIGHEST_ACCURACY)
    updates = solved[..., :channel_width]
    key_weights = solved[..., channel_width:]
    tail_keys = block_keys * jnp.exp(cumulative[..., -1:] - cumulative)[..., None]
    last_decay = jnp.exp(cumulative[..., -1])
    identity = jnp.eye(channel_width, dtype=jnp.float32)

    def advance(state_pair, block_items):
        transition, carried_state = state_pair
        update_index, weight_index, tail_index, last_index = block_items
        fresh_value_rows = update_index - jnp.einsum(
            "xbg,xgp->xbp", weight_index, carried_state, precision=HIGHEST_ACCURACY
        )
        carried_state = carried_state * last_index[:, None, None] + jnp.einsum(
            "tjo,tjw->tow", tail_index, fresh_value_rows, precision=HIGHEST_ACCURACY
        )
        block_move = last_index[:, None, None] * identity - jnp.einsum(
            "hck,hcj->hkj", tail_index, weight_index, precision=HIGHEST_ACCURACY
        )
        transition = jnp.einsum("hij,hjk->hik", block_move, transition, precision=HIGHEST_ACCURACY)
        return ((transition, carried_state), None)

    initial = (
        jnp.broadcast_to(identity, (attention_channels_total, channel_width, channel_width)),
        jnp.zeros((attention_channels_total, channel_width, channel_width), jnp.float32),
    )
    block_items = (
        jnp.moveaxis(updates, 1, 0),
        jnp.moveaxis(key_weights, 1, 0),
        jnp.moveaxis(tail_keys, 1, 0),
        jnp.moveaxis(last_decay, 1, 0),
    )
    (transition, carried_state), _ = lax.scan(advance, initial, block_items)
    return (transition, carried_state)


def read_heads(
    state_cache,
    first_step_probe,
    first_step_address,
    first_step_content,
    first_step_outgate,
    first_step_strength_raw,
    channel_scaling_factor,
):
    seq_count, attention_channels_total, channel_width, _ = state_cache.shape
    carried_state = state_cache.astype(jnp.float32)

    def activate(tensor):
        return jax.nn.silu(tensor.astype(jnp.float32)).reshape(
            seq_count, attention_channels_total, channel_width
        )

    query_rows = activate(first_step_probe)
    address_token_slab = activate(first_step_address)
    address_token_slab = address_token_slab * lax.rsqrt(
        jnp.sum(address_token_slab * address_token_slab, axis=-1, keepdims=True) + EPSILON
    )
    content_token_slab = activate(first_step_content)
    storing_strength = jax.nn.sigmoid(first_step_strength_raw)
    recalled = jnp.einsum(
        "nhk,nhkv->nhv", address_token_slab, carried_state, precision=HIGHEST_ACCURACY
    )
    updated = (
        carried_state
        + storing_strength[..., None, None]
        * address_token_slab[..., :, None]
        * (content_token_slab - recalled)[..., None, :]
    )
    output = jnp.einsum("nhk,nhkv->nhv", query_rows, updated, precision=HIGHEST_ACCURACY)
    normed = (
        output
        * lax.rsqrt(jnp.mean(output * output, axis=-1, keepdims=True) + EPSILON)
        * channel_scaling_factor
    )
    gated_out = normed * activate(first_step_outgate)
    return gated_out.reshape(seq_count, attention_channels_total * channel_width).astype(
        jnp.bfloat16
    )


def matmul_maps(left, right):
    return jnp.einsum("shij,shjk->shik", left, right, precision=HIGHEST_ACCURACY)


def join_pairs(earlier, later):
    return (matmul_maps(later[0], earlier[0]), matmul_maps(later[0], earlier[1]) + later[1])


def per_device(
    layer_source_tokens,
    address_projection,
    content_projection,
    strength_projection,
    fading_driver_projection,
    strength_offset,
    channel_fading_speed,
    added_fading_exponent,
    first_step_probe,
    first_step_address,
    first_step_content,
    first_step_outgate,
    first_step_strength_raw,
    channel_scaling_factor,
    readout_projection,
):
    head_local = channel_fading_speed.shape[0]
    first_head = lax.axis_index("tp") * head_local
    beta_slice = lax.dynamic_slice_in_dim(strength_projection, first_head, head_local, 1)
    alpha_slice = lax.dynamic_slice_in_dim(fading_driver_projection, first_head, head_local, 1)
    seq_count, local_len, model_width = layer_source_tokens.shape
    flat_rows = layer_source_tokens.reshape(seq_count * local_len, model_width)
    key_sum = jnp.dot(
        flat_rows,
        lax.all_gather(address_projection, "sp", axis=0, tiled=True),
        preferred_element_type=jnp.float32,
    )
    value_sum = jnp.dot(
        flat_rows,
        lax.all_gather(content_projection, "sp", axis=0, tiled=True),
        preferred_element_type=jnp.float32,
    )
    beta_sum = jnp.dot(flat_rows, beta_slice, preferred_element_type=jnp.float32)
    alpha_sum = jnp.dot(flat_rows, alpha_slice, preferred_element_type=jnp.float32)
    outgate_raw_scores = (
        jnp.concatenate([beta_sum, alpha_sum], axis=1)
        .astype(jnp.bfloat16)
        .reshape(seq_count, local_len, -1)
    )
    address_vectors = key_sum.astype(jnp.bfloat16).reshape(seq_count, local_len, -1)
    content_vectors = value_sum.astype(jnp.bfloat16).reshape(seq_count, local_len, -1)
    transitions = []
    offsets = []
    for prompt_number in range(seq_count):
        address_token_slab, content_token_slab, storing_strength, fading_exponent = build_arguments(
            address_vectors[prompt_number],
            content_vectors[prompt_number],
            outgate_raw_scores[prompt_number],
            strength_offset,
            channel_fading_speed,
            added_fading_exponent[prompt_number],
            ADDRESS_WIDTH,
        )
        transition, carried_state = range_map(
            address_token_slab, content_token_slab, storing_strength, fading_exponent, BLOCK
        )
        transitions.append(transition)
        offsets.append(carried_state)
    transition = jnp.stack(transitions)
    offset = jnp.stack(offsets)
    identity = jnp.broadcast_to(jnp.eye(ADDRESS_WIDTH, dtype=jnp.float32), transition.shape)
    entered = prefix((transition, offset), "sp", join_pairs, (identity, jnp.zeros_like(offset)))
    leaving = matmul_maps(transition, entered[1]) + offset
    final = broadcast(as_sent(leaving), "sp", lax.axis_size("sp") - 1).astype(leaving.dtype)
    boundary_cache = leaving.astype(jnp.bfloat16)[:, None]
    state_cache = final.astype(jnp.bfloat16)
    heads_read = read_heads(
        state_cache,
        first_step_probe,
        first_step_address,
        first_step_content,
        first_step_outgate,
        first_step_strength_raw,
        channel_scaling_factor,
    )
    group_terms = jnp.dot(
        heads_read, readout_projection, preferred_element_type=jnp.float32
    ).astype(jnp.bfloat16)
    mixed_read = lax.psum(group_terms.astype(jnp.float32).astype(jnp.bfloat16), "tp")
    return (state_cache, mixed_read, boundary_cache)


def solution(mesh):
    return jax.shard_map(
        per_device,
        mesh=mesh,
        in_specs=(
            P(None, "sp", None),
            P("sp", "tp"),
            P("sp", "tp"),
            P(),
            P(),
            P("tp"),
            P("tp"),
            P(None, "sp", "tp"),
            P(None, "tp"),
            P(None, "tp"),
            P(None, "tp"),
            P(None, "tp"),
            P(None, "tp"),
            P(),
            P("tp", "sp"),
        ),
        out_specs=(P(None, "tp", None, None), P(None, "sp"), P(None, "sp", "tp", None, None)),
        check_vma=False,
    )
```

profile of v0, /device:TPU:13, one launch (start us, length us, event | category | flops | bytes accessed | tf_op | source)
XLA Modules:
  0.0 639.6 jit_solution(9558476493292765205)
XLA Ops:
  7.2 0.7 all-gather.5.cloned.1.call-update
  8.0 0.7 all-gather.7.cloned.1.call-update
  8.7 1.2 fusion.11
  9.9 1.2 fusion.12
  11.2 0.8 fusion.121
  13.1 108.3 %all-gather.5.cloned.1.call-done = bf16[4096,1024]{1,0:T(8,128)(2,1)} async-done(((bf16[256,1024]{1,0:T(8,128)(2,1)}), bf16[4096,1024]{1,0:T(8,128)(2,1)}) %all-gather.5.cloned.1.call-update) | async-done | bytes 8388624 | tf_op jit(solution)/shard_map/all_gather | solution.py:226
  121.4 4.6 convolution_convert_fusion.1
  126.4 0.7 fusion.10
  127.2 0.4 fusion.145
  127.5 0.4 fusion.146
  128.7 0.7 fusion.9
  130.2 0.4 fusion.67
  130.6 0.4 fusion.65
  131.0 0.4 fusion.63
  131.4 0.4 convolution_add_fusion.5
  131.8 0.4 fusion.61
  132.2 0.4 fusion.58
  132.6 102.0 %all-gather.7.cloned.1.call-done = bf16[4096,1024]{1,0:T(8,128)(2,1)} async-done(((bf16[256,1024]{1,0:T(8,128)(2,1)}), bf16[4096,1024]{1,0:T(8,128)(2,1)}) %all-gather.7.cloned.1.call-update) | async-done | bytes 8388624 | tf_op jit(solution)/shard_map/all_gather | solution.py:231
  234.6 4.6 convolution_convert_fusion
  239.7 0.5 fusion.32
  240.2 0.6 convolution_bitcast_fusion.1
  241.2 1.2 convolution_add_fusion.3
  242.4 0.8 copy-done.1
  243.2 0.6 fusion.152
  243.7 0.4 fusion.56
  244.5 0.4 fusion.54
  245.0 0.4 convolution_add_fusion.4
  245.3 0.4 fusion.52
  245.7 0.4 fusion.154
  246.1 0.6 convolution_bitcast_fusion
  247.1 1.2 convolution_add_fusion.2
  248.3 0.8 copy-done.2
  249.1 0.8 pad_maximum_fusion.1
  250.1 1.2 convolution_subtract_fusion.1
  251.2 0.6 fusion.72
  251.9 1.2 convolution_subtract_fusion
  253.1 0.6 fusion.70
  253.7 0.8 pad_maximum_fusion
  254.8 105.8 %all-gather.11.cloned.1.call-done = bf16[16,2,8,128,128]{4,3,2,1,0:T(8,128)(2,1)} async-done(((bf16[1,2,8,128,128]{4,3,2,1,0:T(8,128)(2,1)}), bf16[16,2,8,128,128]{4,3,2,1,0:T(8,128)(2,1)}) %all-gather.11.cloned.1.call-update) | async-done | bytes 8388624 | tf_op jit(solution)/shard_map/all_gather | solution.py:17
  360.6 113.7 %all-gather.9.cloned.1.call-done = bf16[16,2,8,128,128]{4,3,2,1,0:T(8,128)(2,1)} async-done(((bf16[1,2,8,128,128]{4,3,2,1,0:T(8,128)(2,1)}), bf16[16,2,8,128,128]{4,3,2,1,0:T(8,128)(2,1)}) %all-gather.9.cloned.1.call-update) | async-done | bytes 8388624 | tf_op jit(solution)/shard_map/all_gather | solution.py:17
  474.3 35.4 %while.9 = (s32[]{:T(128)}, f32[2,8,128,128]{3,2,1,0:T(8,128)S(1)}, s32[]{:T(128)}, bf16[16,2,8,128,128]{4,3,2,1,0:T(8,128)(2,1)}, bf16[16,2,8,128,128]{4,3,2,1,0:T(8,128)(2,1)}, /*index=5*/s32[]{:T(128)}, s32[]{:T(128)}) while((s32[]{:T(128)}, f32[2,8,128,128]{3,2,1,0:T(8,128)S(1)}, s32[]{:T(128)}, ...), condition=%wide.region_5.6_spmd.clone, body=%wide.region_4.5_spmd.clone.sunk | while | flops 403963904 | bytes 6294111 | solution.py:34
  474.4 2.1 fusion.208
  476.6 2.1 fusion.208
  478.8 2.1 fusion.208
  481.1 2.1 fusion.208
  483.3 2.1 fusion.208
  485.5 2.1 fusion.208
  487.7 2.1 fusion.208
  489.9 2.1 fusion.208
  492.1 2.1 fusion.208
  494.3 2.1 fusion.208
  496.6 2.1 fusion.208
  498.8 2.1 fusion.208
  501.0 2.1 fusion.208
  503.2 2.1 fusion.208
  505.4 2.1 fusion.208
  507.6 2.1 fusion.208
  509.8 3.4 broadcast_select_fusion
  513.3 107.3 %all-reduce.2.cloned.1.call-done = bf16[2,8,128,128]{3,2,1,0:T(8,128)(2,1)} async-done(((bf16[2,8,128,128]{3,2,1,0:T(8,128)(2,1)}), bf16[2,8,128,128]{3,2,1,0:T(8,128)(2,1)}) %all-reduce.2.cloned.1.call-update) | async-done | bytes 524304 | tf_op jit(solution)/shard_map/psum | solution.py:43
  620.6 1.6 fusion.155
  622.2 2.2 fusion.16
  624.6 1.2 convolution_convert_fusion.4
  625.8 5.4 psum.15
  631.2 1.9 copy.114
  (83 shorter events, 6.5 us)
Async XLA Ops:
  7.2 1.6 copy-start
  7.2 114.2 %all-gather.5.cloned.1.call-start = ((), (), s32[]{:S(2)}) async-start(), calls=%async_computation | async-start | bytes 8912896 | tf_op jit(solution)/shard_map/all_gather | solution.py:226
  7.9 226.7 %all-gather.7.cloned.1.call-start = ((), (), s32[]{:S(2)}) async-start(), calls=%async_computation.1 | async-start | bytes 8912896 | tf_op jit(solution)/shard_map/all_gather | solution.py:231
  8.7 352.0 %all-gather.11.cloned.1.call-start = ((), (), s32[]{:S(2)}) async-start(), calls=%async_computation.3 | async-start | bytes 8912896 | tf_op jit(solution)/shard_map/all_gather | solution.py:17
  242.3 0.8 copy-start.1
  244.9 9.7 %copy-start.3 = (bf16[2,1024]{1,0:T(2,128)(2,1)S(1)}, bf16[2,1024]{1,0:T(2,128)(2,1)}, u32[]{:S(2)}) copy-start(bf16[2,1024]{1,0:T(2,128)(2,1)} %param.26) | copy-start | bytes 12292
  244.9 9.8 %copy-start.4 = (bf16[2,1024]{1,0:T(2,128)(2,1)S(1)}, bf16[2,1024]{1,0:T(2,128)(2,1)}, u32[]{:S(2)}) copy-start(bf16[2,1024]{1,0:T(2,128)(2,1)} %param.27) | copy-start | bytes 12292
  244.9 9.8 %copy-start.5 = (bf16[2,1024]{1,0:T(2,128)(2,1)S(1)}, bf16[2,1024]{1,0:T(2,128)(2,1)}, u32[]{:S(2)}) copy-start(bf16[2,1024]{1,0:T(2,128)(2,1)} %param.25) | copy-start | bytes 12292
  248.3 0.8 copy-start.2
  250.0 224.3 %all-gather.9.cloned.1.call-start = ((), (), s32[]{:S(2)}) async-start(), calls=%async_computation.2 | async-start | bytes 8912896 | tf_op jit(solution)/shard_map/all_gather | solution.py:17
  254.6 366.1 %all-reduce.2.cloned.1.call-start = ((), (), s32[]{:S(2)}) async-start(), calls=%async_computation.4 | async-start | bytes 1048576 | tf_op jit(solution)/shard_map/psum | solution.py:43
  474.3 38.9 %copy-start.7 = (f32[2,8]{1,0:T(2,128)S(1)}, f32[2,8]{1,0:T(2,128)}, u32[]{:S(2)}) copy-start(f32[2,8]{1,0:T(2,128)} %param.29) | copy-start | bytes 196
  474.3 38.9 %copy-start.6 = (bf16[2,1024]{1,0:T(2,128)(2,1)S(1)}, bf16[2,1024]{1,0:T(2,128)(2,1)}, u32[]{:S(2)}) copy-start(bf16[2,1024]{1,0:T(2,128)(2,1)} %param.28) | copy-start | bytes 12292
  474.3 150.1 %copy-start.8 = (f32[128]{0:T(128)S(1)}, f32[128]{0:T(128)}, u32[]{:S(2)}) copy-start(f32[128]{0:T(128)} %param.30) | copy-start | bytes 1540
Sparse Core Ops, SparseCore 0:
  10.8 110.5 all-gather.4
  124.1 110.4 all-gather.6
  250.1 110.4 all-gather.10
  363.8 110.4 all-gather.8
  513.3 107.2 all-reduce.1
where the time goes:
time: 643 us; the launch traced here: 640 us
  waiting for transfers between devices  539 us (84%)
  matrix products  70.9 us (11%)
  between operations  14.3 us (2%)
    all_gather x2, waiting for transfers between devices, prefix(): lax.all_gather(part.astype(kind), axis)  220 us
    all_gather x1, waiting for transfers between devices, per_device(): lax.all_gather(address_projection, 'sp', axis=0, tiled=True)  108 us
    psum x1, waiting for transfers between devices, broadcast(): return lax.psum(kept, axis)  107 us
    all_gather x1, waiting for transfers between devices, per_device(): lax.all_gather(content_projection, 'sp', axis=0, tiled=True)  102 us
    dot_general x17, matrix products, matmul_maps(): jnp.einsum('shij,shjk->shik', left, right, precision=HIGHEST_ACCURACY)  37.1 us
  transfers between devices with their start and end apart: 5, of which 5 were waited for; matrix products, arithmetic and copies ran while one was open for 3% of the time, Pallas kernels for 0%

commit v1 on v0

--- a/solution.py
+++ b/solution.py
@@ -1,6 +1,8 @@
 import jax
 import jax.numpy as jnp
 from jax import lax
+from jax.experimental import pallas as pl
+from jax.experimental.pallas import tpu as pltpu
 from jax.sharding import PartitionSpec as P
 
 ADDRESS_WIDTH = 128
@@ -281,9 +283,381 @@
     return (state_cache, mixed_read, boundary_cache)
 
 
+MESH = pl.DeviceIdType.MESH
+PIECES = 2
+
+
+def remote(src, dst, send, recv, sp, tp):
+    return pltpu.make_async_remote_copy(
+        src_ref=src,
+        dst_ref=dst,
+        send_sem=send,
+        recv_sem=recv,
+        device_id={"sp": sp, "tp": tp},
+        device_id_type=MESH,
+    )
+
+
+def gather_kernel(
+    peers,
+    tok,
+    wk,
+    wv,
+    add,
+    xall,
+    wall,
+    addall,
+    own_sem,
+    across_send,
+    a_send,
+    b_send,
+    tok_recv,
+    w_send,
+    w_recv,
+    relay_send,
+    relay_recv,
+    add_send,
+    add_recv,
+):
+    s, t = lax.axis_index("sp"), lax.axis_index("tp")
+    ring = peers // 2
+    x, q = s % 2, s // 2
+    half = tok.shape[2] // 2
+    length = tok.shape[1]
+    piece = length // PIECES
+    rows = wk.shape[0]
+    width = ADDRESS_WIDTH
+    columns = pl.ds(pl.multiple_of(t * half, 128), half)
+
+    def place(r):
+        y = r // (ring // 2)
+        z = (1 - y) * r + y * (ring - 1 - r)
+        return 2 * z + y
+
+    y, z = q % 2, q // 2
+    r = (1 - y) * z + y * (ring - 1 - z)
+    after = place((r + 1) % ring)
+    before = place((r + ring - 1) % ring)
+
+    def part(i):
+        return pl.ds(i * piece, piece)
+
+    def token_wait(slot, i):
+        ref = xall.at[slot, part(i)]
+        remote(ref, ref, across_send.at[i], tok_recv.at[slot, i], s, t).wait_recv()
+
+    sent = []
+
+    def go(copy):
+        copy.start()
+        sent.append(copy)
+
+    for i in range(PIECES):
+        go(
+            remote(
+                tok.at[1 - x, part(i), columns],
+                xall.at[s, part(i)],
+                across_send.at[i],
+                tok_recv.at[s, i],
+                2 * q + 1 - x,
+                t,
+            )
+        )
+        go(
+            remote(
+                tok.at[x, part(i), columns],
+                xall.at[s, part(i)],
+                a_send.at[0, i],
+                tok_recv.at[s, i],
+                2 * after + x,
+                t,
+            )
+        )
+    own = pltpu.make_async_copy(tok.at[x, :, columns], xall.at[s], own_sem)
+    own.start()
+
+    side = s // ring
+    row_slot = s % ring
+    spot = pl.ds(pl.multiple_of(row_slot * rows, 16), rows)
+    for off in range(ring):
+        head = (q + off) % ring
+        for kv, w in enumerate((wk, wv)):
+            src = w.at[:, pl.ds(pl.multiple_of(head * width, 128), width)]
+            dst = wall.at[spot, pl.ds(pl.multiple_of((2 * t + kv) * width, 128), width)]
+            copy = remote(
+                src, dst, w_send.at[off, kv], w_recv.at[row_slot, 2 * t + kv], 2 * head + x, side
+            )
+            if off == 0:
+
+                @pl.when(t == side)
+                def _():
+                    pltpu.make_async_copy(src, dst, w_recv.at[row_slot, 2 * t + kv]).start()
+
+                @pl.when(t != side)
+                def _():
+                    copy.start()
+            else:
+                go(copy)
+
+    for off in range(1, peers):
+        to = (s + off) % peers
+        go(remote(add.at[to % 2], addall.at[s], add_send.at[off], add_recv.at[s], to, t))
+    own_add = pltpu.make_async_copy(add.at[x], addall.at[s], add_recv.at[s])
+    own_add.start()
+
+    def relay(m):
+        slot = 2 * m + x
+        block = wall.at[pl.ds(pl.multiple_of(slot * rows, 16), rows)]
+        for c in range(4):
+            one = wall.at[pl.ds(pl.multiple_of(slot * rows, 16), rows), pl.ds(c * width, width)]
+            pltpu.make_async_copy(one, one, w_recv.at[slot, c]).wait()
+        go(remote(block, block, relay_send.at[m], relay_recv.at[slot], 2 * q + 1 - x, t))
+
+    relays = list(range(ring // 2))
+    for k in range(ring - 1):
+        for i in range(PIECES):
+            if k > 0:
+                slot = 2 * place((r - k + ring) % ring) + x
+                token_wait(slot, i)
+                ref = xall.at[slot, part(i)]
+                go(remote(ref, ref, a_send.at[k, i], tok_recv.at[slot, i], 2 * after + x, t))
+            slot = 2 * place((r + k) % ring) + 1 - x
+            token_wait(slot, i)
+            ref = xall.at[slot, part(i)]
+            go(remote(ref, ref, b_send.at[k, i], tok_recv.at[slot, i], 2 * before + x, t))
+        if k >= 2 and relays:
+            relay(relays.pop(0))
+    while relays:
+        relay(relays.pop(0))
+    for i in range(PIECES):
+        token_wait(2 * place((r + 1) % ring) + x, i)
+        token_wait(2 * place((r + ring - 1) % ring) + 1 - x, i)
+    for m in range(ring // 2):
+        slot = 2 * m + 1 - x
+        block = wall.at[pl.ds(pl.multiple_of(slot * rows, 16), rows)]
+        remote(block, block, relay_send.at[m], relay_recv.at[slot], s, t).wait_recv()
+    own.wait()
+    for off in range(peers):
+        slot = (s + off) % peers
+        pltpu.make_async_copy(addall.at[slot], addall.at[slot], add_recv.at[slot]).wait()
+    for copy in sent:
+        copy.wait_send()
+
+    @pl.when(t != side)
+    def _():
+        for kv, w in enumerate((wk, wv)):
+            src = w.at[:, pl.ds(pl.multiple_of(q * width, 128), width)]
+            dst = wall.at[spot, pl.ds(pl.multiple_of((2 * t + kv) * width, 128), width)]
+            remote(
+                src, dst, w_send.at[0, kv], w_recv.at[row_slot, 2 * t + kv], 2 * q + x, side
+            ).wait_send()
+
+
+def gather_inputs(tok, wk, wv, add, peers):
+    seq_count, length, model_width = tok.shape
+    ring = peers // 2
+    heads = add.shape[1]
+    dma = pltpu.SemaphoreType.DMA
+    anywhere = pl.BlockSpec(memory_space=pl.ANY)
+    vmem = pl.BlockSpec(memory_space=pltpu.VMEM)
+    return pl.pallas_call(
+        lambda *refs: gather_kernel(peers, *refs),
+        out_shape=(
+            jax.ShapeDtypeStruct((peers, length, model_width // 2), tok.dtype),
+            jax.ShapeDtypeStruct((model_width // 2, 4 * ADDRESS_WIDTH), wk.dtype),
+            jax.ShapeDtypeStruct((peers, heads, length), add.dtype),
+        ),
+        in_specs=[anywhere] * 4,
+        out_specs=(vmem, vmem, vmem),
+        scratch_shapes=[
+            dma(()),
+            dma((PIECES,)),
+            dma((ring - 1, PIECES)),
+            dma((ring - 1, PIECES)),
+            dma((peers, PIECES)),
+            dma((ring, 2)),
+            dma((ring, 4)),
+            dma((ring // 2,)),
+            dma((ring,)),
+            dma((peers,)),
+            dma((peers,)),
+        ],
+        compiler_params=pltpu.CompilerParams(has_side_effects=True),
+        name="gather_inputs",
+    )(tok, wk, wv, add)
+
+
+def spread_kernel(peers, states, final, bound, f_send, f_recv, b_send, b_recv):
+    s, t = lax.axis_index("sp"), lax.axis_index("tp")
+    ring = peers // 2
+    slot = (s % 2) * ring + s // 2
+    sent = []
+    for send, recv, out, last in ((f_send, f_recv, final, True), (b_send, b_recv, bound, False)):
+        for off in range(1, peers):
+            to = (s + off) % peers
+            copy = remote(
+                states.at[peers - 1 if last else to],
+                out.at[slot],
+                send.at[off],
+                recv.at[slot],
+                to,
+                t,
+            )
+            copy.start()
+            sent.append(copy)
+    final[slot] = states[peers - 1]
+    bound[slot] = states[s]
+    for out, recv in ((final, f_recv), (bound, b_recv)):
+        for off in range(1, peers):
+            other = (s + off) % peers
+            slot_from = (other % 2) * ring + other // 2
+            ref = out.at[slot_from]
+            remote(ref, ref, f_send.at[off], recv.at[slot_from], s, t).wait_recv()
+    for copy in sent:
+        copy.wait_send()
+
+
+def spread_states(states, peers):
+    dma = pltpu.SemaphoreType.DMA
+    vmem = pl.BlockSpec(memory_space=pltpu.VMEM)
+    return pl.pallas_call(
+        lambda *refs: spread_kernel(peers, *refs),
+        out_shape=(jax.ShapeDtypeStruct(states.shape, states.dtype),) * 2,
+        in_specs=[vmem],
+        out_specs=(vmem, vmem),
+        scratch_shapes=[dma((peers,))] * 4,
+        compiler_params=pltpu.CompilerParams(has_side_effects=True),
+        name="spread_states",
+    )(states)
+
+
+def dot32(spec, a, b):
+    return jnp.einsum(spec, a, b, precision=HIGHEST_ACCURACY)
+
+
+def block_states(keys, values, beta, fading):
+    blocks, block, width = keys.shape
+    cumulative = jnp.cumsum(fading, axis=-1)
+    positions = jnp.arange(block)
+    strict = positions[:, None] > positions[None, :]
+    spread_log = jnp.where(strict, cumulative[:, :, None] - cumulative[:, None, :], 0.0)
+    scaled_keys = keys * beta[..., None]
+    inner = dot32("nik,njk->nij", scaled_keys, keys)
+    inverse = unit_inverse(jnp.where(strict, inner * jnp.exp(spread_log), 0.0))
+    targets = jnp.concatenate(
+        [scaled_keys * jnp.exp(cumulative)[..., None], values * beta[..., None]], axis=-1
+    )
+    solved = dot32("nij,njk->nik", inverse, targets)
+    tail = keys * jnp.exp(cumulative[:, -1:] - cumulative)[..., None]
+    maps = dot32("nck,ncj->nkj", tail, solved)
+    last = jnp.exp(cumulative[:, -1])[:, None, None]
+    moves = last * jnp.eye(width, dtype=jnp.float32) - maps[..., :width]
+    pair = jnp.concatenate([moves, maps[..., width:]], axis=-1)
+    zero = jnp.zeros((blocks, width, width), jnp.float32)
+    reach = 1
+    while reach < blocks:
+        late = pair[reach:]
+        joined = dot32("nij,njk->nik", late[..., :width], pair[:-reach])
+        joined = joined + jnp.concatenate([zero[reach:], late[..., width:]], axis=-1)
+        pair = jnp.concatenate([pair[:reach], joined], axis=0)
+        reach *= 2
+    return pair[..., width:]
+
+
+def per_device_heads(
+    layer_source_tokens,
+    address_projection,
+    content_projection,
+    strength_projection,
+    fading_driver_projection,
+    strength_offset,
+    channel_fading_speed,
+    added_fading_exponent,
+    first_step_probe,
+    first_step_address,
+    first_step_content,
+    first_step_outgate,
+    first_step_strength_raw,
+    channel_scaling_factor,
+    readout_projection,
+):
+    peers = lax.axis_size("sp")
+    head_local = channel_fading_speed.shape[0]
+    s, t = lax.axis_index("sp"), lax.axis_index("tp")
+    mine = s // 2
+    _, length, model_width = layer_source_tokens.shape
+    half = model_width // 2
+    width = ADDRESS_WIDTH
+    tokens, weights, added = gather_inputs(
+        layer_source_tokens,
+        address_projection,
+        content_projection,
+        jnp.swapaxes(added_fading_exponent, 1, 2),
+        peers,
+    )
+    flat = tokens.reshape(peers * length, half)
+    gates = jnp.concatenate([strength_projection, fading_driver_projection], axis=1)
+    gates = lax.dynamic_slice_in_dim(gates, t * half, half, 0)
+    wide = jnp.dot(flat, weights, preferred_element_type=jnp.float32)
+    gate_sum = jnp.dot(flat, gates, preferred_element_type=jnp.float32)
+    gate_sum = lax.psum(gate_sum, "tp").astype(jnp.bfloat16).astype(jnp.float32)
+    kept = lax.dynamic_slice_in_dim(wide, t * 2 * width, 2 * width, 1)
+    given = lax.dynamic_slice_in_dim(wide, (1 - t) * 2 * width, 2 * width, 1)
+    wide = kept + lax.ppermute(given, "tp", ((0, 1), (1, 0)))
+    wide = wide.astype(jnp.bfloat16).astype(jnp.float32).reshape(peers, length, 2 * width)
+    acted = jax.nn.silu(wide)
+    keys = acted[..., :width]
+    keys = keys * lax.rsqrt(jnp.sum(keys * keys, axis=-1, keepdims=True) + EPSILON)
+    values = acted[..., width:]
+    head = t * head_local + mine
+    total_heads = strength_projection.shape[1]
+    beta_logit = lax.dynamic_slice_in_dim(gate_sum, head, 1, 1).reshape(peers, length)
+    alpha_logit = lax.dynamic_slice_in_dim(gate_sum, total_heads + head, 1, 1).reshape(
+        peers, length
+    )
+    beta = jax.nn.sigmoid(beta_logit + lax.dynamic_index_in_dim(strength_offset, mine, 0))
+    added_own = lax.dynamic_index_in_dim(added, mine, 1, keepdims=False)
+    speed = lax.dynamic_index_in_dim(channel_fading_speed, mine, 0)
+    fading = added_own - speed * jax.nn.softplus(alpha_logit)
+    states = block_states(keys, values, beta, fading).astype(jnp.bfloat16)
+    final, bound = spread_states(states, peers)
+    state_cache = final.reshape(2, head_local, width, width)
+    boundary_cache = bound.reshape(2, 1, head_local, width, width)
+    heads_read = read_heads(
+        state_cache,
+        first_step_probe,
+        first_step_address,
+        first_step_content,
+        first_step_outgate,
+        first_step_strength_raw,
+        channel_scaling_factor,
+    )
+    group_terms = jnp.dot(
+        heads_read, readout_projection, preferred_element_type=jnp.float32
+    ).astype(jnp.bfloat16)
+    return (state_cache, lax.psum(group_terms, "tp"), boundary_cache)
+
+
+def by_heads(mesh):
+    def choose(*args):
+        seq_count, length, model_width = args[0].shape
+        peers, heads = lax.axis_size("sp"), args[6].shape[0]
+        fits = (
+            lax.axis_size("tp") == 2
+            and seq_count == 2
+            and peers == 2 * heads
+            and heads % 2 == 0
+            and length == BLOCK
+            and args[1].shape[0] * peers == model_width
+        )
+        return per_device_heads(*args) if fits else per_device(*args)
+
+    return choose
+
+
 def solution(mesh):
     return jax.shard_map(
-        per_device,
+        by_heads(mesh),
         mesh=mesh,
         in_specs=(
             P(None, "sp", None),

time: 643 us -> 159 us (0.25)
  waiting for transfers between devices: 539 us -> 0.01 us
  Pallas kernels: 0 us -> 107 us
  matrix products: 70.9 us -> 30.1 us
  between operations: 14.3 us -> 1.16 us
    all_gather x4 -> x0, waiting for transfers between devices: 430 us -> none  [the longest x2 220 us: prefix(): lax.all_gather(part.astype(kind), axis)]
    psum x1 -> x0, waiting for transfers between devices: 107 us -> none  [broadcast(): return lax.psum(kept, axis)]
    pallas_call x0 -> x2, Pallas kernels: none -> 107 us  [the longest x1 75.6 us: gather_inputs(): pl.pallas_call(lambda *refs: gather_kernel(peers, *refs), out_shape=(jax....]
    dot_general x34 -> x10, matrix products: 59.3 us -> 19.7 us  [the longest x7 10.8 us: dot32(): return jnp.einsum(spec, a, b, precision=HIGHEST_ACCURACY)]
  transfers between devices with their start and end apart: 5 -> 1, of which waited for: 5 -> 0; matrix products, arithmetic and copies ran while one was open for 3% -> 5% of each run, Pallas kernels for 0% -> 0%
where the time goes in v1:
time: 159 us; the launch traced here: 158 us
  Pallas kernels  107 us (67%)
  matrix products  30.1 us (19%)
  blocking collectives  8.03 us (5%)
  other arithmetic  5.97 us (4%)
  local copies, waits for them, and re-layouts  5.35 us (3%)
    pallas_call x1, Pallas kernels, gather_inputs(): pl.pallas_call(lambda *refs: gather_kernel(peers, *refs), out_shape=(jax....  75.6 us
    pallas_call x1, Pallas kernels, spread_states(): pl.pallas_call(lambda *refs: spread_kernel(peers, *refs), out_shape=(jax....  31 us
    dot_general x7, matrix products, dot32(): return jnp.einsum(spec, a, b, precision=HIGHEST_ACCURACY)  10.8 us
    dot_general x1, matrix products, per_device_heads(): wide = jnp.dot(flat, weights, preferred_element_type=jnp.float32)  5.19 us
    psum x1, blocking collectives, per_device_heads(): gate_sum = lax.psum(gate_sum, 'tp').astype(jnp.bfloat16).astype(jnp.float32)  4.03 us
    psum x1, blocking collectives, per_device_heads(): return (state_cache, lax.psum(group_terms, 'tp'), boundary_cache)  3.99 us
    dot_general x1, matrix products, per_device_heads(): gate_sum = jnp.dot(flat, gates, preferred_element_type=jnp.float32)  3.54 us
    dot_general x5, matrix products, unit_inverse(): jnp.matmul(result, identity + power_term, precision=HIGHEST_ACCURACY)  3.27 us
  transfers between devices with their start and end apart: 1, of which 0 were waited for; matrix products, arithmetic and copies ran while one was open for 5% of the time, Pallas kernels for 0%

profile of v1, /device:TPU:13, one launch (start us, length us, event | category | flops | bytes accessed | tf_op | source)
XLA Modules:
  0.0 158.2 jit_solution(5293772689817914342)
XLA Ops:
  0.6 0.0 copy-start
  0.7 75.6 %gather_inputs.1 = (bf16[16,64,2048]{2,1,0:T(8,128)(2,1)}, bf16[2048,512]{1,0:T(8,128)(2,1)}, f32[16,8,64]{2,1,0:T(8,128)}) custom-call(bf16[2,64,4096]{2,1,0:T(8,128)(2,1)} %refs_0_.1, bf16[256,1024]{1,0:T(8,128)(2,1)} %refs_1_.1, bf16[256,1024]{1,0:T(8,128)(2,1)} %refs_2_.1, f32[2,8,64]{2,1,0:T(8,128)} %bitcast.89), custom_call_target="tpu_custom_call" | custom-call | tf_op jit(solution)/shard_map/gather_inputs/pallas_call | solution.py:463
  76.3 5.2 %fusion.78 = f32[1024,512]{1,0:T(8,128)S(1)} fusion(bf16[1024,2048]{1,0:T(8,128)(2,1)} %bitcast.77, bf16[2048,512]{1,0:T(8,128)(2,1)} %get-tuple-element.10), kind=kOutput, calls=%fused_computation.131 | convolution fusion | flops 2147483648 | bytes 8388608 | tf_op jit(solution)/shard_map/dot_general | solution.py:601
  81.5 0.0 copy-start.3
  81.5 0.0 copy-start.4
  81.5 1.1 constant_dynamic-slice_fusion
  82.6 1.0 collective-permute-start
  83.6 0.0 copy-start.11
  83.6 0.0 copy-start.12
  83.6 0.0 copy-start.5
  83.6 0.0 copy-start.6
  83.7 0.0 copy-start.8
  83.7 3.5 %fusion.48 = f32[1024,32]{0,1:T(8,128)S(1)} fusion(bf16[1024,2048]{1,0:T(8,128)(2,1)} %bitcast.78, s32[]{:T(128)S(6)} %select_n.40, bf16[4096,16]{0,1:T(8,128)(2,1)S(1)} %copy-done.3, bf16[4096,16]{0,1:T(8,128)(2,1)S(1)} %copy-done.4), kind=kOutput, calls=%fused_computation.72 | convolution fusion | flops 134479872 | bytes 4587524 | tf_op jit(solution)/shard_map/dot_general | solution.py:602
  87.2 4.0 %all-reduce.5 = bf16[1024,32]{0,1:T(8,128)(2,1)S(1)} all-reduce(f32[1024,32]{0,1:T(8,128)S(1)} %fusion.48), channel_id=1, replica_groups=mesh['sp'=16,'tp'=2] {'tp'}, use_global_device_ids=true, to_apply=%region_0.1 | all-reduce | flops 32768 | bytes 196608 | tf_op jit(solution)/shard_map/psum | solution.py:603
  91.3 0.6 dynamic_slice.33
  91.9 0.7 divide_reduce_fusion
  92.6 0.1 reshape.135
  92.7 0.8 constant_dynamic-slice_fusion.1
  93.5 0.6 dynamic_slice.27
  94.1 0.7 fusion.65
  94.8 0.2 reduce_window_sum.11
  95.0 0.2 slice_reduce_fusion
  95.2 0.1 fusion.67
  95.4 0.1 reshape.147
  95.5 0.1 subtract_exponential_fusion
  95.6 0.1 broadcast_multiply_fusion
  95.7 1.4 add_convert_fusion
  97.1 0.3 convert_multiply_fusion
  97.4 0.2 multiply_reduce_fusion
  97.6 0.5 multiply_multiply_fusion
  98.1 1.3 fusion.10
  99.4 0.6 fusion.79
  100.1 0.6 fusion.80
  100.7 0.7 fusion.34
  101.4 0.6 fusion.81
  102.0 0.7 fusion.32
  102.7 0.6 fusion.82
  103.3 0.7 fusion.30
  104.0 0.6 convolution_add_fusion.1
  104.7 0.7 fusion.28
  105.3 0.6 fusion.83
  106.0 1.0 fusion.14
  107.0 2.5 %fusion.37 = f32[16,128,256]{2,1,0:T(8,128)S(1)} fusion(f32[16,64,256]{2,1,0:T(8,128)S(1)} %fusion.14, f32[16,64,256]{2,1,0:T(8,128)S(1)} %convert_multiply_fusion, f32[16,64]{1,0:T(8,128)S(1)} %get-tuple-element.29, f32[16,64]{1,0:T(8,128)S(1)} %add_rsqrt_fusion), kind=kOutput, calls=%fused_computation.57 | convolution fusion | flops 402915328 | bytes 3686400 | tf_op jit(solution)/shard_map/nck,ncj->nkj/dot_general | solution.py:535
  109.5 0.1 slice.111
  109.6 0.2 fusion.77
  109.8 1.8 %pad_add_fusion = f32[15,128,256]{2,1,0:T(8,128)S(1)} fusion(f32[15,128,128]{2,1,0:T(8,128)S(1)} %slice.111, f32[16,128,128]{2,1,0:T(8,128)S(1)} %get-tuple-element.26, f32[16,128,128]{2,1,0:T(8,128)S(1)} %get-tuple-element.25), kind=kOutput, calls=%fused_computation.6 | convolution fusion | flops 755957760 | bytes 5046272 | tf_op jit(solution)/shard_map/nij,njk->nik/dot_general | solution.py:535
  111.6 0.2 fusion
  111.8 0.1 slice.115
  111.9 1.7 %pad_add_fusion.1 = f32[14,128,256]{2,1,0:T(8,128)S(1)} fusion(f32[14,128,128]{2,1,0:T(8,128)S(1)} %slice.115, f32[16,128,256]{2,1,0:T(8,128)S(1)} %fusion, f32[15,128,256]{2,1,0:T(8,128)S(1)} %pad_add_fusion), kind=kOutput, calls=%fused_computation.9 | convolution fusion | flops 705101824 | bytes 5505024 | tf_op jit(solution)/shard_map/nij,njk->nik/dot_general | solution.py:535
  113.7 0.1 slice.117
  113.7 1.5 pad_add_fusion.2
  115.2 0.2 fusion.76
  115.4 1.0 fusion.9
  116.5 0.0 copy-start.10
  116.5 0.9 pad_maximum_fusion.10.refs_0_
  117.4 31.0 %spread_states.1 = (bf16[16,128,128]{2,1,0:T(8,128)(2,1)}, bf16[16,128,128]{2,1,0:T(8,128)(2,1)}) custom-call(bf16[16,128,128]{2,1,0:T(8,128)(2,1)} %pad_maximum_fusion.10.refs_0_), custom_call_target="tpu_custom_call" | custom-call | tf_op jit(solution)/shard_map/spread_states/pallas_call | solution.py:523
  148.4 1.6 %fusion.84 = f32[2,8,1,128]{3,2,1,0:T(1,128)S(1)} fusion(f32[2,8,128,1]{2,3,1,0:T(1,128)S(1)} %bitcast.85, bf16[2,8,128,128]{3,2,1,0:T(8,128)(2,1)} %bitcast.79), kind=kOutput, calls=%fused_computation.137 | convolution fusion | flops 3145728 | bytes 540672 | tf_op jit(solution)/shard_map/nhk,nhkv->nhv/dot_general | solution.py:174
  150.1 2.2 %fusion.18 = f32[2,8,1,128]{3,2,1,0:T(1,128)S(1)} fusion(f32[2,8,128,1]{2,3,1,0:T(1,128)S(1)} %bitcast.90, bf16[2,8,128,128]{3,2,1,0:T(8,128)(2,1)} %bitcast.80, f32[2,8,128]{2,1,0:T(8,128)S(1)} %bitcast_subtract_fusion, f32[2,8,128]{2,1,0:T(8,128)S(1)} %get-tuple-element.21), kind=kOutput, calls=%fused_computation.34 | convolution fusion | flops 3932160 | bytes 557056 | tf_op jit(solution)/shard_map/nhk,nhkv->nhv/dot_general | solution.py:183
  152.2 0.1 multiply_reduce_fusion.1
  152.3 0.1 fusion.68
  152.4 0.2 convolution_convert_fusion
  152.6 4.0 %psum.15 = bf16[2,256]{1,0:T(2,128)(2,1)} all-reduce(bf16[2,256]{1,0:T(2,128)(2,1)S(1)} %convolution_convert_fusion), channel_id=1, replica_groups=mesh['sp'=16,'tp'=2] {'tp'}, use_global_device_ids=true, to_apply=%region_5.6 | all-reduce | flops 512 | bytes 2048 | tf_op jit(solution)/shard_map/psum | solution.py:638
  156.6 0.8 copy.46
  157.4 0.8 copy.47
  (34 shorter events, 0.2 us)
Async XLA Ops:
  0.6 151.8 %copy-start = (bf16[1024,256]{1,0:T(8,128)(2,1)S(1)}, bf16[1024,256]{1,0:T(8,128)(2,1)}, u32[]{:S(2)}) copy-start(bf16[1024,256]{1,0:T(8,128)(2,1)} %param.29) | copy-start | bytes 1572868
  81.5 2.1 %copy-start.3 = (bf16[4096,16]{0,1:T(8,128)(2,1)S(1)}, bf16[4096,16]{0,1:T(8,128)(2,1)}, u32[]{:S(2)}) copy-start(bf16[4096,16]{0,1:T(8,128)(2,1)} %param.18) | copy-start | bytes 393220
  81.5 2.1 %copy-start.4 = (bf16[4096,16]{0,1:T(8,128)(2,1)S(1)}, bf16[4096,16]{0,1:T(8,128)(2,1)}, u32[]{:S(2)}) copy-start(bf16[4096,16]{0,1:T(8,128)(2,1)} %param.19) | copy-start | bytes 393220
  82.6 13.1 %collective-permute-start = (f32[1024,256]{1,0:T(8,128)}, f32[1024,256]{1,0:T(8,128)}, u32[]{:S(2)}, u32[]{:S(2)}) collective-permute-start(f32[1024,256]{1,0:T(8,128)} %constant_dynamic-slice_fusion), channel_id=1, source_target_pairs={{0,1},{1,0},{2,3},{3,2},{4,5},{5,4},{6,7},{7,6},{8,9},{9,8},{10,11... | collective-permute-start | bytes 3145736 | tf_op jit(solution)/shard_map/ppermute | solution.py:606
  83.6 7.7 %copy-start.11 = (f32[8]{0:T(128)S(1)}, f32[8]{0:T(128)}, u32[]{:S(2)}) copy-start(f32[8]{0:T(128)} %param.20) | copy-start | bytes 100
  83.6 9.9 %copy-start.12 = (f32[8]{0:T(128)S(1)}, f32[8]{0:T(128)}, u32[]{:S(2)}) copy-start(f32[8]{0:T(128)} %param.21) | copy-start | bytes 100
  83.6 11.6 %copy-start.5 = (bf16[2,1024]{1,0:T(2,128)(2,1)S(1)}, bf16[2,1024]{1,0:T(2,128)(2,1)}, u32[]{:S(2)}) copy-start(bf16[2,1024]{1,0:T(2,128)(2,1)} %param.24) | copy-start | bytes 12292
  83.6 11.7 %copy-start.6 = (bf16[2,1024]{1,0:T(2,128)(2,1)S(1)}, bf16[2,1024]{1,0:T(2,128)(2,1)}, u32[]{:S(2)}) copy-start(bf16[2,1024]{1,0:T(2,128)(2,1)} %param.23) | copy-start | bytes 12292
  83.6 11.7 %copy-start.9 = (f32[2,8]{1,0:T(2,128)S(1)}, f32[2,8]{1,0:T(2,128)}, u32[]{:S(2)}) copy-start(f32[2,8]{1,0:T(2,128)} %param.27) | copy-start | bytes 196
  83.7 11.8 %copy-start.7 = (bf16[2,1024]{1,0:T(2,128)(2,1)S(1)}, bf16[2,1024]{1,0:T(2,128)(2,1)}, u32[]{:S(2)}) copy-start(bf16[2,1024]{1,0:T(2,128)(2,1)} %param.25) | copy-start | bytes 12292
  83.7 11.8 %copy-start.8 = (bf16[2,1024]{1,0:T(2,128)(2,1)S(1)}, bf16[2,1024]{1,0:T(2,128)(2,1)}, u32[]{:S(2)}) copy-start(bf16[2,1024]{1,0:T(2,128)(2,1)} %param.26) | copy-start | bytes 12292
  116.5 35.9 %copy-start.10 = (f32[128]{0:T(128)S(1)}, f32[128]{0:T(128)}, u32[]{:S(2)}) copy-start(f32[128]{0:T(128)} %param.28) | copy-start | bytes 1540
  148.4 8.2 %copy-start.1 = (bf16[16,128,128]{2,1,0:T(8,128)(2,1)S(1)}, bf16[16,128,128]{2,1,0:T(8,128)(2,1)}, u32[]{:S(2)}) copy-start(bf16[16,128,128]{2,1,0:T(8,128)(2,1)} %get-tuple-element.11) | copy-start | bytes 1572868
  148.4 9.0 %copy-start.2 = (bf16[16,128,128]{2,1,0:T(8,128)(2,1)S(1)}, bf16[16,128,128]{2,1,0:T(8,128)(2,1)}, u32[]{:S(2)}) copy-start(bf16[16,128,128]{2,1,0:T(8,128)(2,1)} %get-tuple-element.12) | copy-start | bytes 1572868

commit v2 on v1

--- a/solution.py
+++ b/solution.py
@@ -304,9 +304,14 @@
     wk,
     wv,
     add,
+    gates,
+    out,
+    addall,
     xall,
     wall,
-    addall,
+    keep,
+    give,
+    got,
     own_sem,
     across_send,
     a_send,
@@ -318,6 +323,8 @@
     relay_recv,
     add_send,
     add_recv,
+    give_send,
+    give_recv,
 ):
     s, t = lax.axis_index("sp"), lax.axis_index("tp")
     ring = peers // 2
@@ -377,21 +384,22 @@
     own.start()
 
     side = s // ring
+    other = (t + side) % 2
     row_slot = s % ring
     spot = pl.ds(pl.multiple_of(row_slot * rows, 16), rows)
     for off in range(ring):
         head = (q + off) % ring
         for kv, w in enumerate((wk, wv)):
             src = w.at[:, pl.ds(pl.multiple_of(head * width, 128), width)]
-            dst = wall.at[spot, pl.ds(pl.multiple_of((2 * t + kv) * width, 128), width)]
+            dst = wall.at[spot, pl.ds(pl.multiple_of((2 * other + kv) * width, 128), width)]
             copy = remote(
-                src, dst, w_send.at[off, kv], w_recv.at[row_slot, 2 * t + kv], 2 * head + x, side
+                src, dst, w_send.at[off, kv], w_recv.at[row_slot, 2 * other + kv], 2 * head + x, side
             )
             if off == 0:
 
                 @pl.when(t == side)
                 def _():
-                    pltpu.make_async_copy(src, dst, w_recv.at[row_slot, 2 * t + kv]).start()
+                    pltpu.make_async_copy(src, dst, w_recv.at[row_slot, 2 * other + kv]).start()
 
                 @pl.when(t != side)
                 def _():
@@ -429,31 +437,64 @@
             relay(relays.pop(0))
     while relays:
         relay(relays.pop(0))
-    for i in range(PIECES):
-        token_wait(2 * place((r + 1) % ring) + x, i)
-        token_wait(2 * place((r + ring - 1) % ring) + 1 - x, i)
     for m in range(ring // 2):
         slot = 2 * m + 1 - x
         block = wall.at[pl.ds(pl.multiple_of(slot * rows, 16), rows)]
         remote(block, block, relay_send.at[m], relay_recv.at[slot], s, t).wait_recv()
     own.wait()
+
+    def project(g):
+        slots = []
+        for k in (2 * g, 2 * g + 1):
+            slots.append(2 * place((r - k + ring) % ring) + x)
+            slots.append(2 * place((r + k) % ring) + 1 - x)
+        rows_in = jnp.concatenate([xall[slot] for slot in slots], axis=0)
+        wide = jnp.dot(rows_in, wall[...], preferred_element_type=jnp.float32)
+        logits = jnp.dot(rows_in, gates[...], preferred_element_type=jnp.float32)
+        for i, slot in enumerate(slots):
+            part_of = slice(i * length, (i + 1) * length)
+            keep[slot, :, : 2 * width] = wide[part_of, : 2 * width]
+            keep[slot, :, 2 * width :] = logits[part_of]
+            give[slot, :, : 2 * width] = wide[part_of, 2 * width :]
+            give[slot, :, 2 * width :] = logits[part_of]
+        for slot in slots:
+            remote(
+                give.at[slot], got.at[slot], give_send.at[slot], give_recv.at[slot], s, 1 - t
+            ).start()
+
+    lax.fori_loop(0, ring // 2 - 1, lambda g, c: (project(g), c)[1], 0)
+    for i in range(PIECES):
+        token_wait(2 * place((r + 1) % ring) + x, i)
+        token_wait(2 * place((r + ring - 1) % ring) + 1 - x, i)
+    project(ring // 2 - 1)
     for off in range(peers):
         slot = (s + off) % peers
         pltpu.make_async_copy(addall.at[slot], addall.at[slot], add_recv.at[slot]).wait()
     for copy in sent:
         copy.wait_send()
 
+    def finish(slot, c):
+        copy = remote(
+            give.at[slot], got.at[slot], give_send.at[slot], give_recv.at[slot], s, 1 - t
+        )
+        copy.wait_recv()
+        out[slot] = (keep[slot] + got[slot]).astype(out.dtype)
+        copy.wait_send()
+        return c
+
+    lax.fori_loop(0, peers, finish, 0)
+
     @pl.when(t != side)
     def _():
         for kv, w in enumerate((wk, wv)):
             src = w.at[:, pl.ds(pl.multiple_of(q * width, 128), width)]
-            dst = wall.at[spot, pl.ds(pl.multiple_of((2 * t + kv) * width, 128), width)]
+            dst = wall.at[spot, pl.ds(pl.multiple_of((2 * other + kv) * width, 128), width)]
             remote(
-                src, dst, w_send.at[0, kv], w_recv.at[row_slot, 2 * t + kv], 2 * q + x, side
+                src, dst, w_send.at[0, kv], w_recv.at[row_slot, 2 * other + kv], 2 * q + x, side
             ).wait_send()
 
 
-def gather_inputs(tok, wk, wv, add, peers):
+def gather_inputs(tok, wk, wv, add, gates, peers):
     seq_count, length, model_width = tok.shape
     ring = peers // 2
     heads = add.shape[1]
@@ -463,13 +504,17 @@
     return pl.pallas_call(
         lambda *refs: gather_kernel(peers, *refs),
         out_shape=(
-            jax.ShapeDtypeStruct((peers, length, model_width // 2), tok.dtype),
-            jax.ShapeDtypeStruct((model_width // 2, 4 * ADDRESS_WIDTH), wk.dtype),
+            jax.ShapeDtypeStruct((peers, length, 2 * ADDRESS_WIDTH + gates.shape[1]), tok.dtype),
             jax.ShapeDtypeStruct((peers, heads, length), add.dtype),
         ),
-        in_specs=[anywhere] * 4,
-        out_specs=(vmem, vmem, vmem),
+        in_specs=[anywhere] * 4 + [vmem],
+        out_specs=(vmem, vmem),
         scratch_shapes=[
+            pltpu.VMEM((peers, length, model_width // 2), tok.dtype),
+            pltpu.VMEM((model_width // 2, 4 * ADDRESS_WIDTH), wk.dtype),
+            pltpu.VMEM((peers, length, 2 * ADDRESS_WIDTH + gates.shape[1]), jnp.float32),
+            pltpu.VMEM((peers, length, 2 * ADDRESS_WIDTH + gates.shape[1]), jnp.float32),
+            pltpu.VMEM((peers, length, 2 * ADDRESS_WIDTH + gates.shape[1]), jnp.float32),
             dma(()),
             dma((PIECES,)),
             dma((ring - 1, PIECES)),
@@ -481,38 +526,62 @@
             dma((ring,)),
             dma((peers,)),
             dma((peers,)),
+            dma((peers,)),
+            dma((peers,)),
         ],
         compiler_params=pltpu.CompilerParams(has_side_effects=True),
         name="gather_inputs",
-    )(tok, wk, wv, add)
+    )(tok, wk, wv, add, gates)
 
 
 def spread_kernel(peers, states, final, bound, f_send, f_recv, b_send, b_recv):
     s, t = lax.axis_index("sp"), lax.axis_index("tp")
     ring = peers // 2
     slot = (s % 2) * ring + s // 2
+    x, q = s % 2, s // 2
+    y, z = q % 2, q // 2
+    deep = ring // 2
     sent = []
-    for send, recv, out, last in ((f_send, f_recv, final, True), (b_send, b_recv, bound, False)):
-        for off in range(1, peers):
-            to = (s + off) % peers
-            copy = remote(
-                states.at[peers - 1 if last else to],
-                out.at[slot],
-                send.at[off],
-                recv.at[slot],
-                to,
-                t,
-            )
-            copy.start()
-            sent.append(copy)
+
+    def go(copy):
+        copy.start()
+        sent.append(copy)
+
+    def pass_on(slot_of, src, to, sem):
+        go(remote(src, final.at[slot_of], f_send.at[sem], f_recv.at[slot_of], to, t))
+
+    def arrived(slot_of):
+        ref = final.at[slot_of]
+        remote(ref, ref, f_send.at[0], f_recv.at[slot_of], s, t).wait_recv()
+
+    own = states.at[peers - 1]
+    y_peer, x_peer = 4 * z + 2 * (1 - y) + x, 2 * q + 1 - x
+    for off in range(1, deep):
+        pass_on(slot, own, 4 * ((z + off) % deep) + 2 * y + x, off)
+    pass_on(slot, own, y_peer, deep)
+    pass_on(slot, own, x_peer, 2 * deep)
     final[slot] = states[peers - 1]
+    for off in range(1, peers):
+        to = (s + off) % peers
+        go(remote(states.at[to], bound.at[slot], b_send.at[off], b_recv.at[slot], to, t))
     bound[slot] = states[s]
-    for out, recv in ((final, f_recv), (bound, b_recv)):
-        for off in range(1, peers):
-            other = (s + off) % peers
-            slot_from = (other % 2) * ring + other // 2
-            ref = out.at[slot_from]
-            remote(ref, ref, f_send.at[off], recv.at[slot_from], s, t).wait_recv()
+    for off in range(1, deep):
+        come = x * ring + 2 * ((z + off) % deep) + y
+        arrived(come)
+        pass_on(come, final.at[come], y_peer, deep + off)
+        pass_on(come, final.at[come], x_peer, 2 * deep + off)
+    for off in range(deep):
+        come = x * ring + 2 * ((z + off) % deep) + 1 - y
+        arrived(come)
+        pass_on(come, final.at[come], x_peer, 3 * deep + off)
+    for off in range(ring):
+        arrived((1 - x) * ring + (q + off) % ring)
+    for off in range(1, peers):
+        other = (s + off) % peers
+        ref = bound.at[(other % 2) * ring + other // 2]
+        remote(
+            ref, ref, b_send.at[off], b_recv.at[(other % 2) * ring + other // 2], s, t
+        ).wait_recv()
     for copy in sent:
         copy.wait_send()
 
@@ -532,7 +601,19 @@
 
 
 def dot32(spec, a, b):
-    return jnp.einsum(spec, a, b, precision=HIGHEST_ACCURACY)
+    return jnp.einsum(spec, a, b, precision=lax.Precision.HIGH)
+
+
+def block_inverse(lower):
+    order = lower.shape[-1]
+    identity = jnp.eye(order, dtype=jnp.float32)
+    result, power = identity - lower, lower
+    reached = 2
+    while reached < order:
+        power = dot32("nij,njk->nik", power, power)
+        result = dot32("nij,njk->nik", result, identity + power)
+        reached = reached * 2
+    return result
 
 
 def block_states(keys, values, beta, fading):
@@ -543,7 +624,7 @@
     spread_log = jnp.where(strict, cumulative[:, :, None] - cumulative[:, None, :], 0.0)
     scaled_keys = keys * beta[..., None]
     inner = dot32("nik,njk->nij", scaled_keys, keys)
-    inverse = unit_inverse(jnp.where(strict, inner * jnp.exp(spread_log), 0.0))
+    inverse = block_inverse(jnp.where(strict, inner * jnp.exp(spread_log), 0.0))
     targets = jnp.concatenate(
         [scaled_keys * jnp.exp(cumulative)[..., None], values * beta[..., None]], axis=-1
     )
@@ -588,23 +669,21 @@
     _, length, model_width = layer_source_tokens.shape
     half = model_width // 2
     width = ADDRESS_WIDTH
-    tokens, weights, added = gather_inputs(
+    gates = jnp.concatenate([strength_projection, fading_driver_projection], axis=1)
+    gates = lax.dynamic_slice_in_dim(gates, t * half, half, 0)
+    gate_count = gates.shape[1]
+    gates = jnp.pad(gates, ((0, 0), (0, -gate_count % 128)))
+    projected, added = gather_inputs(
         layer_source_tokens,
         address_projection,
         content_projection,
         jnp.swapaxes(added_fading_exponent, 1, 2),
+        gates,
         peers,
     )
-    flat = tokens.reshape(peers * length, half)
-    gates = jnp.concatenate([strength_projection, fading_driver_projection], axis=1)
-    gates = lax.dynamic_slice_in_dim(gates, t * half, half, 0)
-    wide = jnp.dot(flat, weights, preferred_element_type=jnp.float32)
-    gate_sum = jnp.dot(flat, gates, preferred_element_type=jnp.float32)
-    gate_sum = lax.psum(gate_sum, "tp").astype(jnp.bfloat16).astype(jnp.float32)
-    kept = lax.dynamic_slice_in_dim(wide, t * 2 * width, 2 * width, 1)
-    given = lax.dynamic_slice_in_dim(wide, (1 - t) * 2 * width, 2 * width, 1)
-    wide = kept + lax.ppermute(given, "tp", ((0, 1), (1, 0)))
-    wide = wide.astype(jnp.bfloat16).astype(jnp.float32).reshape(peers, length, 2 * width)
+    projected = projected.astype(jnp.float32)
+    wide = projected[..., : 2 * width]
+    gate_sum = projected[..., 2 * width :].reshape(peers * length, -1)
     acted = jax.nn.silu(wide)
     keys = acted[..., :width]
     keys = keys * lax.rsqrt(jnp.sum(keys * keys, axis=-1, keepdims=True) + EPSILON)

time: 159 us -> 137 us (0.86); the launches traced: 158 us -> 134 us
  matrix products: 30.1 us -> 14.2 us
  Pallas kernels: 107 us -> 101 us
  blocking collectives: 8.03 us -> 5.01 us
  local copies, waits for them, and re-layouts: 5.35 us -> 7.2 us
    dot_general x19 -> x17, matrix products: 26.1 us -> 10.2 us  [dot32(): return jnp.einsum(spec, a, b, precision=lax.Precision.HIGH)]
    pallas_call x1, Pallas kernels: 31 us -> 22.3 us  [spread_states(): pl.pallas_call(lambda *refs: spread_kernel(peers, *refs), out_shape=(jax....]
    psum x1 -> x0, blocking collectives: 4.03 us -> none  [per_device_heads(): gate_sum = lax.psum(gate_sum, 'tp').astype(jnp.bfloat16).astype(jnp.float32)]
    pallas_call x1, Pallas kernels: 75.6 us -> 78.6 us  [gather_inputs(): pl.pallas_call(lambda *refs: gather_kernel(peers, *refs), out_shape=(jax....]
  transfers between devices with their start and end apart: 1 -> 0, of which waited for: 0 -> 0; matrix products, arithmetic and copies ran while one was open for 5% -> 0% of each run, Pallas kernels for 0% -> 0%
where the time goes in v2:
time: 137 us; the launch traced here: 134 us
  Pallas kernels  101 us (74%)
  matrix products  14.2 us (10%)
  local copies, waits for them, and re-layouts  7.2 us (5%)
  other arithmetic  5.88 us (4%)
  blocking collectives  5.01 us (4%)
    pallas_call x1, Pallas kernels, gather_inputs(): pl.pallas_call(lambda *refs: gather_kernel(peers, *refs), out_shape=(jax....  78.6 us
    pallas_call x1, Pallas kernels, spread_states(): pl.pallas_call(lambda *refs: spread_kernel(peers, *refs), out_shape=(jax....  22.3 us
    dot_general x17, matrix products, dot32(): return jnp.einsum(spec, a, b, precision=lax.Precision.HIGH)  10.2 us
    psum x1, blocking collectives, per_device_heads(): return (state_cache, lax.psum(group_terms, 'tp'), boundary_cache)  5.01 us

profile of v2, /device:TPU:13, one launch (start us, length us, event | category | flops | bytes accessed | tf_op | source)
XLA Modules:
  0.0 134.3 jit_solution(11826619893871027325)
XLA Ops:
  0.6 0.0 copy-start
  0.7 0.9 fusion.44
  1.6 0.3 copy.34
  1.9 0.9 pad.8.refs_4_
  2.8 78.6 %gather_inputs.1 = (bf16[16,64,384]{2,1,0:T(8,128)(2,1)}, f32[16,8,64]{2,1,0:T(8,128)}) custom-call(bf16[2,64,4096]{2,1,0:T(8,128)(2,1)} %refs_0_.1, bf16[256,1024]{1,0:T(8,128)(2,1)} %refs_1_.1, bf16[256,1024]{1,0:T(8,128)(2,1)} %refs_2_.1, f32[2,8,64]{2,1,0:T(8,128)} %bitcast.82, bf16[2048,128]{1,0:T(8,128)(2,1)} %pad.8.refs_4_), custom_call_target="tpu_custom_call" | custom-call | tf_op jit(solution)/shard_map/gather_inputs/pallas_call | solution.py:504
  81.4 0.0 copy-start.10
  81.4 1.1 slice.114
  82.5 0.5 constant_dynamic-slice_fusion
  83.0 0.1 reshape.129
  83.1 0.9 constant_dynamic-slice_fusion.1
  83.9 0.6 dynamic_slice.22
  84.5 0.7 fusion.60
  85.2 0.2 reduce_window_sum.11
  85.4 0.2 slice_reduce_fusion
  85.6 0.2 convert_element_type.54
  85.8 0.0 copy-start.11
  85.8 0.3 divide_multiply_fusion
  86.1 0.2 multiply_reduce_fusion
  86.3 0.1 subtract_exponential_fusion
  86.3 0.2 copy.36
  86.5 0.6 dynamic_slice.25
  87.1 0.7 divide_reduce_fusion
  87.8 0.1 reshape.137
  87.9 0.5 multiply_multiply_fusion
  88.4 0.9 fusion.10
  89.3 0.4 fusion.71
  89.6 0.4 fusion.31
  90.0 0.4 fusion.72
  90.4 0.4 fusion.29
  90.8 0.4 fusion.73
  91.1 0.4 fusion.27
  91.5 0.4 fusion.74
  91.9 0.4 fusion.25
  92.3 0.4 convolution_add_fusion.1
  92.6 0.4 fusion.75
  93.0 0.6 fusion.11
  93.6 1.4 %fusion.34 = f32[16,128,256]{2,1,0:T(8,128)S(1)} fusion(f32[16,64,256]{2,1,0:T(8,128)S(1)} %fusion.11, f32[16,64,256]{2,1,0:T(8,128)S(1)} %divide_multiply_fusion, f32[16,64]{1,0:T(8,128)S(1)} %get-tuple-element.30, f32[16,64]{1,0:T(8,128)S(1)} %get-tuple-element.32), kind=kOutput, calls=%fused_computation.52 | convolution fusion | flops 201588736 | bytes 3686400 | tf_op jit(solution)/shard_map/nck,ncj->nkj/dot_general | solution.py:604
  95.0 0.2 fusion.70
  95.3 0.1 slice.121
  95.4 1.0 pad_add_fusion
  96.4 0.2 fusion
  96.6 0.1 slice.125
  96.7 1.1 pad_add_fusion.1
  97.8 0.1 slice.127
  97.9 0.9 pad_add_fusion.2
  98.8 0.4 fusion.69
  99.2 0.0 copy-start.4
  99.2 0.0 copy-start.8
  99.2 0.7 fusion.9
  99.9 0.0 copy-start.5
  99.9 0.0 copy-start.6
  99.9 0.0 copy-start.7
  99.9 0.9 pad_maximum_fusion.10.refs_0_
  100.9 22.3 %spread_states.1 = (bf16[16,128,128]{2,1,0:T(8,128)(2,1)}, bf16[16,128,128]{2,1,0:T(8,128)(2,1)}) custom-call(bf16[16,128,128]{2,1,0:T(8,128)(2,1)} %pad_maximum_fusion.10.refs_0_), custom_call_target="tpu_custom_call" | custom-call | tf_op jit(solution)/shard_map/spread_states/pallas_call | solution.py:592
  123.3 0.1 fusion.62
  123.4 0.1 broadcast_multiply_fusion
  123.4 1.6 %fusion.76 = f32[2,8,1,128]{3,2,1,0:T(1,128)S(1)} fusion(f32[2,8,128,1]{2,3,1,0:T(1,128)S(1)} %bitcast.78, bf16[2,8,128,128]{3,2,1,0:T(8,128)(2,1)} %bitcast.73), kind=kOutput, calls=%fused_computation.127 | convolution fusion | flops 3145728 | bytes 540672 | tf_op jit(solution)/shard_map/nhk,nhkv->nhv/dot_general | solution.py:174
  125.2 2.2 %fusion.15 = f32[2,8,1,128]{3,2,1,0:T(1,128)S(1)} fusion(f32[2,8,128,1]{2,3,1,0:T(1,128)S(1)} %bitcast.83, bf16[2,8,128,128]{3,2,1,0:T(8,128)(2,1)} %bitcast.74, f32[2,8,128]{2,1,0:T(8,128)S(1)} %bitcast_subtract_fusion, f32[2,8,128]{2,1,0:T(8,128)S(1)} %get-tuple-element.20), kind=kOutput, calls=%fused_computation.29 | convolution fusion | flops 3932160 | bytes 557056 | tf_op jit(solution)/shard_map/nhk,nhkv->nhv/dot_general | solution.py:183
  127.3 0.1 multiply_reduce_fusion.1
  127.5 0.1 fusion.63
  127.6 0.2 convolution_convert_fusion
  127.7 5.0 %psum.7 = bf16[2,256]{1,0:T(2,128)(2,1)} all-reduce(bf16[2,256]{1,0:T(2,128)(2,1)S(1)} %convolution_convert_fusion), channel_id=1, replica_groups=mesh['sp'=16,'tp'=2] {'tp'}, use_global_device_ids=true, to_apply=%region_4.5 | all-reduce | flops 512 | bytes 2048 | tf_op jit(solution)/shard_map/psum | solution.py:717
  132.7 0.8 copy.58
  133.5 0.8 copy.59
  (30 shorter events, 0.2 us)
Async XLA Ops:
  0.6 126.9 %copy-start = (bf16[1024,256]{1,0:T(8,128)(2,1)S(1)}, bf16[1024,256]{1,0:T(8,128)(2,1)}, u32[]{:S(2)}) copy-start(bf16[1024,256]{1,0:T(8,128)(2,1)} %param.29) | copy-start | bytes 1572868
  81.4 2.5 %copy-start.10 = (f32[8]{0:T(128)S(1)}, f32[8]{0:T(128)}, u32[]{:S(2)}) copy-start(f32[8]{0:T(128)} %param.21) | copy-start | bytes 100
  81.4 4.2 %copy-start.1 = (bf16[16,64,384]{2,1,0:T(8,128)(2,1)S(1)}, bf16[16,64,384]{2,1,0:T(8,128)(2,1)}, u32[]{:S(2)}) copy-start(bf16[16,64,384]{2,1,0:T(8,128)(2,1)} %get-tuple-element.8) | copy-start | bytes 2359300
  85.8 0.8 copy-start.11
  99.2 24.0 %copy-start.4 = (bf16[2,1024]{1,0:T(2,128)(2,1)S(1)}, bf16[2,1024]{1,0:T(2,128)(2,1)}, u32[]{:S(2)}) copy-start(bf16[2,1024]{1,0:T(2,128)(2,1)} %param.24) | copy-start | bytes 12292
  99.2 24.1 %copy-start.8 = (f32[2,8]{1,0:T(2,128)S(1)}, f32[2,8]{1,0:T(2,128)}, u32[]{:S(2)}) copy-start(f32[2,8]{1,0:T(2,128)} %param.27) | copy-start | bytes 196
  99.9 25.2 %copy-start.5 = (bf16[2,1024]{1,0:T(2,128)(2,1)S(1)}, bf16[2,1024]{1,0:T(2,128)(2,1)}, u32[]{:S(2)}) copy-start(bf16[2,1024]{1,0:T(2,128)(2,1)} %param.25) | copy-start | bytes 12292
  99.9 25.2 %copy-start.6 = (bf16[2,1024]{1,0:T(2,128)(2,1)S(1)}, bf16[2,1024]{1,0:T(2,128)(2,1)}, u32[]{:S(2)}) copy-start(bf16[2,1024]{1,0:T(2,128)(2,1)} %param.23) | copy-start | bytes 12292
  99.9 27.5 %copy-start.7 = (bf16[2,1024]{1,0:T(2,128)(2,1)S(1)}, bf16[2,1024]{1,0:T(2,128)(2,1)}, u32[]{:S(2)}) copy-start(bf16[2,1024]{1,0:T(2,128)(2,1)} %param.26) | copy-start | bytes 12292
  99.9 27.5 %copy-start.9 = (f32[128]{0:T(128)S(1)}, f32[128]{0:T(128)}, u32[]{:S(2)}) copy-start(f32[128]{0:T(128)} %param.28) | copy-start | bytes 1540
  123.2 9.6 %copy-start.2 = (bf16[16,128,128]{2,1,0:T(8,128)(2,1)S(1)}, bf16[16,128,128]{2,1,0:T(8,128)(2,1)}, u32[]{:S(2)}) copy-start(bf16[16,128,128]{2,1,0:T(8,128)(2,1)} %get-tuple-element.9) | copy-start | bytes 1572868
  123.2 10.3 %copy-start.3 = (bf16[16,128,128]{2,1,0:T(8,128)(2,1)S(1)}, bf16[16,128,128]{2,1,0:T(8,128)(2,1)}, u32[]{:S(2)}) copy-start(bf16[16,128,128]{2,1,0:T(8,128)(2,1)} %get-tuple-element.10) | copy-start | bytes 1572868
